TPU v7x, 32 devices: a whole 2x2x4 slice. The times are simulated.
32 devices in a mesh: rep: 4 (over z), fs: 2 (over y), tp: 4 (over x, core).
Axes of the slice: x: 2, y: 2, z: 4, core: 2. Of those that a mesh axis runs over, the one named last changes fastest.
Arguments:
- tokens: bfloat16 [3072, 2048], P('rep', 'fs'), may hold values from -6 to 6
- gate_pre: bfloat16 [3072, 6144], P('rep', 'tp'), may hold values from -6 to 6
- up_pre: bfloat16 [3072, 6144], P('rep', 'tp'), may hold values from -6 to 6
- hidden_grad: bfloat16 [3072, 6144], P('rep', 'tp'), may hold values from -0.75 to 0.75
- gate_weight: bfloat16 [2048, 6144], P('fs', 'tp'), may hold values from -0.125 to 0.125
- up_weight: bfloat16 [2048, 6144], P('fs', 'tp'), may hold values from -0.125 to 0.125
- gate_taps: float32 [3, 6144], P(None, 'tp'), may hold values from -3.5 to 3.5
- up_taps: float32 [3, 6144], P(None, 'tp'), may hold values from -3.5 to 3.5
- gate_bias: float32 [6144], P('tp'), may hold values from -4 to 4
- up_bias: float32 [6144], P('tp'), may hold values from -4 to 4
Outputs:
- input_grad: bfloat16 [3072, 2048], P('rep', 'fs')
- gate_weight_grad: float32 [2048, 6144], P('fs', 'tp')
- up_weight_grad: float32 [2048, 6144], P('fs', 'tp')
- gate_taps_grad: float32 [3, 6144], P(None, 'tp')
- up_taps_grad: float32 [3, 6144], P(None, 'tp')
- gate_bias_grad: float32 [6144], P('tp')
- up_bias_grad: float32 [6144], P('tp')
All inputs are finite; a program needn't handle non-finite values.
Results may differ from a plain program's by a relative error of at most 0.017.
Values may be sent and summed in bfloat16 or wider, within the bound.
A program may use at most 64 MiB of HBM per device.

v0:
```python
import jax
import jax.numpy as jnp
from jax import lax
from jax.sharding import PartitionSpec as P


def causal_mix(signal, tap_weights):
    tap_count = tap_weights.shape[0]
    length = signal.shape[0]
    padded = jnp.pad(signal, ((tap_count - 1, 0), (0, 0)))
    mixed = padded[0:length] * tap_weights[0]
    for offset in range(1, tap_count):
        mixed = mixed + padded[offset : offset + length] * tap_weights[offset]
    return mixed


def mix_back(signal, tap_weights):
    tap_count = tap_weights.shape[0]
    length = signal.shape[0]
    padded = jnp.pad(signal, ((0, tap_count - 1), (0, 0)))
    begin = tap_count - 1
    mixed = padded[begin : begin + length] * tap_weights[0]
    for offset in range(1, tap_count):
        begin = tap_count - 1 - offset
        mixed = mixed + padded[begin : begin + length] * tap_weights[offset]
    return mixed


def tap_terms(grad_signal, signal, tap_count):
    length = signal.shape[0]
    padded = jnp.pad(signal, ((tap_count - 1, 0), (0, 0)))
    return jnp.stack(
        [
            jnp.sum(grad_signal * padded[offset : offset + length], axis=0)
            for offset in range(tap_count)
        ]
    )


def backward_terms(gate_pre, up_pre, hidden_grad, gate_taps, up_taps, gate_bias, up_bias):
    gate_float = gate_pre.astype(jnp.float32)
    up_float = up_pre.astype(jnp.float32)
    gate_mixed = causal_mix(gate_float, gate_taps) + gate_bias
    up_mixed = causal_mix(up_float, up_taps) + up_bias
    logistic = jax.nn.sigmoid(gate_mixed)
    cotangent = hidden_grad.astype(jnp.float32)
    gate_delta = cotangent * up_mixed * logistic * (1.0 + gate_mixed * (1.0 - logistic))
    up_delta = cotangent * gate_mixed * logistic
    gate_back = mix_back(gate_delta, gate_taps).astype(jnp.bfloat16)
    up_back = mix_back(up_delta, up_taps).astype(jnp.bfloat16)
    tap_count = gate_taps.shape[0]
    return (
        gate_back,
        up_back,
        tap_terms(gate_delta, gate_float, tap_count),
        tap_terms(up_delta, up_float, tap_count),
        jnp.sum(gate_delta, axis=0),
        jnp.sum(up_delta, axis=0),
    )


def per_device(
    tokens,
    gate_pre,
    up_pre,
    hidden_grad,
    gate_weight,
    up_weight,
    gate_taps,
    up_taps,
    gate_bias,
    up_bias,
):
    gate_back, up_back, gate_tap_part, up_tap_part, gate_bias_part, up_bias_part = backward_terms(
        gate_pre, up_pre, hidden_grad, gate_taps, up_taps, gate_bias, up_bias
    )
    feature_dims = (((1,), (1,)), ((), ()))
    token_dims = (((0,), (0,)), ((), ()))
    full_partial = lax.dot_general(
        gate_back, gate_weight, feature_dims, preferred_element_type=jnp.float32
    ) + lax.dot_general(up_back, up_weight, feature_dims, preferred_element_type=jnp.float32)
    own_columns = lax.psum_scatter(
        full_partial.astype(jnp.bfloat16), "tp", scatter_dimension=1, tiled=True
    )
    result = lax.all_gather(own_columns, "tp", axis=1, tiled=True)
    gate_local = lax.dot_general(tokens, gate_back, token_dims, preferred_element_type=jnp.float32)
    up_local = lax.dot_general(tokens, up_back, token_dims, preferred_element_type=jnp.float32)
    summed_grads = (
        lax.psum(gate_local.astype(jnp.bfloat16), "rep").astype(jnp.float32),
        lax.psum(up_local.astype(jnp.bfloat16), "rep").astype(jnp.float32),
        lax.psum(gate_tap_part.astype(jnp.bfloat16), "rep").astype(jnp.float32),
        lax.psum(up_tap_part.astype(jnp.bfloat16), "rep").astype(jnp.float32),
        lax.psum(gate_bias_part.astype(jnp.bfloat16), "rep").astype(jnp.float32),
        lax.psum(up_bias_part.astype(jnp.bfloat16), "rep").astype(jnp.float32),
    )
    gate_weight_grad, up_weight_grad, gate_taps_grad, up_taps_grad, gate_bias_grad, up_bias_grad = (
        summed_grads
    )
    return (
        result,
        gate_weight_grad,
        up_weight_grad,
        gate_taps_grad,
        up_taps_grad,
        gate_bias_grad,
        up_bias_grad,
    )


def solution(mesh):
    return jax.shard_map(
        per_device,
        mesh=mesh,
        in_specs=(
            P("rep", "fs"),
            P("rep", "tp"),
            P("rep", "tp"),
            P("rep", "tp"),
            P("fs", "tp"),
            P("fs", "tp"),
            P(None, "tp"),
            P(None, "tp"),
            P("tp"),
            P("tp"),
        ),
        out_specs=(
            P("rep", "fs"),
            P("fs", "tp"),
            P("fs", "tp"),
            P(None, "tp"),
            P(None, "tp"),
            P("tp"),
            P("tp"),
        ),
        check_vma=False,
    )
```

profile of v0, /device:TPU:0, one launch (start us, length us, event | category | flops | bytes accessed | tf_op | source)
XLA Modules:
  0.0 329.4 jit_solution(4718363927047613101)
XLA Ops:
  8.0 0.0 copy-start
  8.0 0.0 reduce-scatter.2.cloned.1.call-start
  8.1 0.0 copy-start.3
  8.1 1.0 slice_reduce_fusion.2
  9.1 1.0 slice_reduce_fusion.5
  10.0 2.3 convert_element_type.66
  12.3 0.0 copy-done.3
  12.4 0.0 copy-start.2
  12.4 0.0 copy-start.7
  12.4 0.6 convert_element_type.65
  13.0 1.0 copy-done.2
  14.0 0.0 copy-done.7
  14.0 0.0 copy-start.8
  14.0 5.8 %fusion.5 = (bf16[1536]{0:T(1024)(128)(2,1)S(1)}, bf16[1536]{0:T(1024)(128)(2,1)S(1)}, bf16[1536]{0:T(1024)(128)(2,1)S(1)}, bf16[1536]{0:T(1024)(128)(2,1)S(1)},...) fusion(bf16[768,1536]{1,0:T(8,128)(2,1)S(1)} %copy-done.3, f32[768,1536]{1,0:T(8,128)S(1)} %convert_element_type.65, ...), kind=kLoop, calls=%fused_computation.32 | loop fusion | flops 23586816 | bytes 23629824 | tf_op jit(solution)/shard_map/reduce_sum | solution.py:58
  19.8 0.0 copy-done.8
  19.8 10.3 %fusion.6 = (bf16[1536]{0:T(1024)(128)(2,1)S(1)}, bf16[1536]{0:T(1024)(128)(2,1)S(1)}, bf16[1536]{0:T(1024)(128)(2,1)S(1)}, bf16[1536]{0:T(1024)(128)(2,1)S(1)},...) fusion(bf16[768,1536]{1,0:T(8,128)(2,1)} %param.11, f32[768,1536]{1,0:T(8,128)S(1)} %convert_element_type.66, ...), kind=kLoop, calls=%fused_computation.33 | loop fusion | flops 35383296 | bytes 30707712 | tf_op jit(solution)/shard_map/reduce_sum | solution.py:57
  30.1 5.9 %add_convert_fusion.1 = bf16[768,1536]{1,0:T(8,128)(2,1)S(1)} fusion(f32[768,1536]{1,0:T(8,128)} %get-tuple-element.40, f32[1536]{0:T(1024)S(1)} %get-tuple-element.30, f32[1536]{0:T(1024)S(1)} %get-tuple-element.31, f32[1536]{0:T(1024)S(1)} %get-tuple-element.29), kind=kLoop, calls=%fused_computation.12 | loop fusion | flops 7077888 | bytes 7096320 | tf_op jit(solution)/shard_map/convert_element_type | solution.py:49
  36.1 0.0 copy-done
  36.1 0.0 copy-start.6
  36.1 0.0 copy-start.4
  36.1 0.0 copy-start.9
  36.1 2.6 fusion.9
  38.7 0.0 copy-done.6
  38.7 0.0 copy-done.4
  38.8 0.8 copy-done.9
  39.5 3.7 %add_convert_fusion.2 = bf16[768,1024]{1,0:T(8,128)(2,1)} fusion(f32[768,1024]{1,0:T(8,128)S(1)} %fusion.9, bf16[768,1536]{1,0:T(8,128)(2,1)S(1)} %copy-done.4, bf16[1024,1536]{1,0:T(8,128)(2,1)S(1)} %copy-done.9), kind=kOutput, calls=%fused_computation.23 | convolution fusion | flops 2417491968 | bytes 10223616 | tf_op jit(solution)/shard_map/dot_general | solution.py:81
  43.2 0.0 reduce-scatter.2.cloned.1.call-update
  43.3 0.0 all-gather.2.cloned.1.call-start
  43.3 30.9 %reduce-scatter.2.cloned.1.call-done = bf16[768,256]{1,0:T(8,128)(2,1)} async-done(((bf16[768,1024]{1,0:T(8,128)(2,1)}), bf16[768,256]{1,0:T(8,128)(2,1)}) %reduce-scatter.2.cloned.1.call-update) | async-done | bytes 393232 | tf_op jit(solution)/shard_map/reduce_scatter | solution.py:82
  74.2 0.0 all-gather.2.cloned.1.call-update
  74.2 0.0 copy-start.5
  74.2 0.0 all-reduce.8.cloned.1.call-start
  74.3 0.0 copy-start.10
  74.3 6.6 %fusion.3 = bf16[1024,1536]{0,1:T(8,128)(2,1)} fusion(bf16[768,1536]{1,0:T(8,128)(2,1)} %copy-done.6, bf16[768,1024]{1,0:T(8,128)(2,1)} %param.10), kind=kOutput, calls=%fused_computation.21 | convolution fusion | flops 2417491968 | bytes 7077888 | tf_op jit(solution)/shard_map/dot_general | solution.py:86
  80.9 0.0 copy-done.5
  80.9 0.0 copy-done.10
  80.9 4.0 %fusion.4 = bf16[1024,1536]{0,1:T(8,128)(2,1)} fusion(bf16[768,1536]{1,0:T(8,128)(2,1)S(1)} %copy-done.5, bf16[768,1024]{1,0:T(8,128)(2,1)S(1)} %copy-done.10), kind=kOutput, calls=%fused_computation.22 | convolution fusion | flops 2417491968 | bytes 7077888 | tf_op jit(solution)/shard_map/dot_general | solution.py:87
  84.9 0.0 all-reduce.8.cloned.1.call-update
  85.0 0.1 pad_maximum_fusion
  85.1 21.1 %all-reduce.4 = (bf16[3,1536]{1,0:T(4,128)(2,1)S(1)}, bf16[3,1536]{1,0:T(4,128)(2,1)S(1)}, bf16[1536]{0:T(1024)(128)(2,1)S(1)}, bf16[1536]{0:T(1024)(128)(2,1)S(1)}) all-reduce(bf16[3,1536]{1,0:T(4,128)(2,1)S(1)} %get-tuple-element.42, bf16[3,1536]{1,0:T(4,128)(2,1)S(1)} %get-tuple-element.43, ...), channel_id=1, replica_groups=mesh['rep'=4,'fs'=2,'tp'=4] {'rep'}, use_global_device_ids=true, to_apply=%region_6.7 | all-reduce | flops 12288 | bytes 49152 | tf_op jit(solution)/shard_map/psum | solution.py:91
  106.2 0.6 convert_element_type.79
  106.8 0.6 convert_element_type.81
  107.4 0.6 convert_element_type.76
  108.0 0.6 convert_element_type.77
  108.6 0.0 all-gather.2.cloned.1.call-done
  108.6 199.7 %all-reduce.8.cloned.1.call-done = (bf16[1024,1536]{0,1:T(8,128)(2,1)}, bf16[1024,1536]{0,1:T(8,128)(2,1)}) async-done(((bf16[1024,1536]{0,1:T(8,128)(2,1)}, bf16[1024,1536]{0,1:T(8,128)(2,1)}), (bf16[1024,1536]{0,1:T(8,128)(2,1)}, bf16[1024,1536]{0,1:T(8,128)(2,1)})) %all-reduce.8.cloned.1.call-update) | async-done | bytes 6291472 | tf_op jit(solution)/shard_map/psum | solution.py:89
  308.3 5.4 %copy.17 = f32[1024,1536]{1,0:T(8,128)} copy(bf16[1024,1536]{0,1:T(8,128)(2,1)} %get-tuple-element.36) | data formatting | bytes 9437184
  313.7 0.0 copy-start.1
  313.7 5.5 %copy.18 = f32[1024,1536]{1,0:T(8,128)} copy(bf16[1024,1536]{0,1:T(8,128)(2,1)} %get-tuple-element.37) | data formatting | bytes 9437184
  319.2 2.7 copy.22
  321.9 0.0 copy-done.1
  (6 shorter events, 0.0 us)
Async XLA Ops:
  8.0 28.1 %copy-start = (bf16[1024,1536]{1,0:T(8,128)(2,1)S(1)}, bf16[1024,1536]{1,0:T(8,128)(2,1)}, u32[]{:S(2)}) copy-start(bf16[1024,1536]{1,0:T(8,128)(2,1)} %param.14) | copy-start | bytes 9437188
  8.0 66.2 %reduce-scatter.2.cloned.1.call-start = ((), (), s32[]{:S(2)}) async-start(), calls=%async_computation.1 | async-start | bytes 1966080 | tf_op jit(solution)/shard_map/reduce_scatter | solution.py:82
  8.1 4.3 %copy-start.3 = (bf16[768,1536]{1,0:T(8,128)(2,1)S(1)}, bf16[768,1536]{1,0:T(8,128)(2,1)}, u32[]{:S(2)}) copy-start(bf16[768,1536]{1,0:T(8,128)(2,1)} %param.12) | copy-start | bytes 7077892
  12.4 1.7 copy-start.2
  12.4 1.7 copy-start.7
  14.0 5.8 %copy-start.8 = (f32[1536]{0:T(1024)S(1)}, f32[1536]{0:T(1024)}, u32[]{:S(2)}) copy-start(f32[1536]{0:T(1024)} %param.19) | copy-start | bytes 18436
  36.1 2.7 copy-start.6
  36.1 2.7 copy-start.4
  36.1 3.4 %copy-start.9 = (bf16[1024,1536]{1,0:T(8,128)(2,1)S(1)}, bf16[1024,1536]{1,0:T(8,128)(2,1)}, u32[]{:S(2)}) copy-start(bf16[1024,1536]{1,0:T(8,128)(2,1)} %param.15) | copy-start | bytes 9437188
  43.3 65.4 %all-gather.2.cloned.1.call-start = ((), (), s32[]{:S(2)}) async-start(), calls=%async_computation.2 | async-start | bytes 1966080 | tf_op jit(solution)/shard_map/all_gather | solution.py:85
  74.2 6.7 %copy-start.5 = (bf16[768,1536]{1,0:T(8,128)(2,1)S(1)}, bf16[768,1536]{1,0:T(8,128)(2,1)}, u32[]{:S(2)}) copy-start(bf16[768,1536]{1,0:T(8,128)(2,1)} %get-tuple-element.41) | copy-start | bytes 7077892
  74.2 234.1 %all-reduce.8.cloned.1.call-start = ((), (), s32[]{:S(2)}) async-start(), calls=%async_computation.3 | async-start | bytes 12582912 | tf_op jit(solution)/shard_map/psum | solution.py:89
  74.3 6.6 %copy-start.10 = (bf16[768,1024]{1,0:T(8,128)(2,1)S(1)}, bf16[768,1024]{1,0:T(8,128)(2,1)}, u32[]{:S(2)}) copy-start(bf16[768,1024]{1,0:T(8,128)(2,1)} %param.10) | copy-start | bytes 4718596
  313.7 8.2 %copy-start.1 = (bf16[1024,1536]{1,0:T(8,128)(2,1)S(1)}, bf16[1024,1536]{1,0:T(8,128)(2,1)}, u32[]{:S(2)}) copy-start(bf16[1024,1536]{1,0:T(8,128)(2,1)} %param.14) | copy-start | bytes 9437188
Sparse Core Ops, SparseCore 0:
  43.4 30.7 reduce-scatter.1
  75.7 19.8 all-gather.1
Sparse Core Ops, SparseCore 1:
  85.0 223.3 all-reduce.7
where the time goes:
time: 330 us; the launch traced here: 329 us
  waiting for transfers between devices  231 us (70%)
  other arithmetic  27.4 us (8%)
  blocking collectives  21.1 us (6%)
  local copies, waits for them, and re-layouts  17.4 us (5%)
  matrix products  17 us (5%)
  between operations  15.7 us (5%)
    psum x1, waiting for transfers between devices, per_device(): lax.psum(gate_local.astype(jnp.bfloat16), 'rep').astype(jnp.float32)  200 us
    reduce_scatter x1, waiting for transfers between devices, per_device(): lax.psum_scatter(full_partial.astype(jnp.bfloat16), 'tp', scatter_dimensi...  30.9 us
    psum x1, blocking collectives, per_device(): lax.psum(gate_tap_part.astype(jnp.bfloat16), 'rep').astype(jnp.float32)  21.1 us
    unnamed x25, local copies, waits for them, and re-layouts  15.4 us
    reduce_sum x1, other arithmetic, backward_terms(): jnp.sum(gate_delta, axis=0)  10.3 us
  transfers between devices with their start and end apart: 3, of which 2 were waited for; matrix products, arithmetic and copies ran while one was open for 4% of the time, Pallas kernels for 0%

commit v1 on v0

v1 whole, which is shorter than its diff:
```python
import functools

import jax
import jax.numpy as jnp
from jax import lax
from jax.experimental import pallas as pl
from jax.experimental.pallas import tpu as pltpu
from jax.sharding import PartitionSpec as P

MESH = pl.DeviceIdType.MESH
CW = 128
NQ = 4
PAD = 8
F32 = jnp.float32
BF16 = jnp.bfloat16


def schedule(blocks, rep_count):
    warm = min(3, blocks)
    done = warm + (blocks - warm + 1) // 2
    steps = max(blocks + rep_count - 1, done + rep_count, done + 3)
    return warm, done, steps


def fused(
    rep_count,
    tp_count,
    tokens,
    gate_pre,
    up_pre,
    hidden,
    gate_weight,
    up_weight,
    gate_taps,
    up_taps,
    gate_bias,
    up_bias,
    grad_out,
    gate_out,
    up_out,
    small_out,
    tok,
    tok_t,
    gpre,
    upre,
    hid,
    gw,
    uw,
    gpad,
    upad,
    gdel,
    udel,
    back,
    acc,
    own,
    from_left,
    from_right,
    to_right,
    to_left,
    out_stage,
    term,
    term_in,
    final,
    small,
    small_from_left,
    small_from_right,
    small_to_right,
    small_to_left,
    load_sem,
    weight_sem,
    send_r,
    recv_r,
    send_l,
    recv_l,
    out_sem,
    scatter_send,
    scatter_recv,
    gather_send,
    gather_recv,
    final_sem,
    small_sem,
):
    z = lax.axis_index("rep")
    me = lax.axis_index("tp")
    length, hidden_cols = gate_pre.shape
    width = tokens.shape[1]
    blocks = hidden_cols // CW
    rows_q = width // NQ
    taps = gate_taps.shape[0]
    warm, done, steps = schedule(blocks, rep_count)
    has_left = z > 0
    has_right = z < rep_count - 1

    def columns(b):
        return pl.ds(pl.multiple_of(b * CW, CW), CW)

    def load(which, b):
        src = (gate_pre, up_pre, hidden)[which]
        dst = (gpre, upre, hid)[which]
        return pltpu.make_async_copy(
            src.at[:, columns(b)], dst.at[b], load_sem.at[which, b]
        )

    token_copy = pltpu.make_async_copy(tokens, tok, weight_sem.at[0])
    weight_copies = (
        pltpu.make_async_copy(gate_weight, gw, weight_sem.at[1]),
        pltpu.make_async_copy(up_weight, uw, weight_sem.at[2]),
    )
    for which in range(3):
        load(which, 0).start()
    token_copy.start()

    def start_load(b, carry):
        for which in range(3):
            load(which, b).start()
        return carry

    lax.fori_loop(1, blocks, start_load, 0)
    for copy in weight_copies:
        copy.start()

    barrier = pltpu.get_barrier_semaphore()

    @pl.when(has_left)
    def _():
        pl.semaphore_signal(barrier, inc=1, device_id={"rep": z - 1}, device_id_type=MESH)

    @pl.when(has_right)
    def _():
        pl.semaphore_signal(barrier, inc=1, device_id={"rep": z + 1}, device_id_type=MESH)

    for d in range(1, tp_count):
        peer = lax.rem(me + d, tp_count)
        pl.semaphore_signal(barrier, inc=1, device_id={"tp": peer}, device_id_type=MESH)

    @pl.when(z == 0)
    def _():
        small_from_left[...] = jnp.zeros_like(small_from_left)

        def clear(c, carry):
            from_left[c] = jnp.zeros((rows_q, 2 * CW), BF16)
            return carry

        lax.fori_loop(0, blocks * NQ, clear, 0)

    @pl.when(z == rep_count - 1)
    def _():
        small_from_right[...] = jnp.zeros_like(small_from_right)

        def clear(c, carry):
            from_right[c] = jnp.zeros((rows_q, 2 * CW), BF16)
            return carry

        lax.fori_loop(0, blocks * NQ, clear, 0)

    zero_rows = jnp.zeros((PAD, CW), F32)
    gpad[0:PAD, :] = zero_rows
    upad[0:PAD, :] = zero_rows
    gdel[length : length + PAD, :] = zero_rows
    udel[length : length + PAD, :] = zero_rows
    acc[...] = jnp.zeros_like(acc)

    token_copy.wait()
    for i in range(width // CW):
        tok_t[i * CW : (i + 1) * CW, :] = tok[:, i * CW : (i + 1) * CW].T

    pl.semaphore_wait(
        barrier,
        jnp.where(has_left, 1, 0) + jnp.where(has_right, 1, 0) + (tp_count - 1),
    )

    row_tile = 128 if length % 128 == 0 else length

    def folded(x):
        return jnp.sum(x.reshape(x.shape[0] // 8, 8, CW), axis=0)

    def compute(b, carry):
        for which in range(3):
            load(which, b).wait()
        cols = columns(b)
        gt = [gate_taps[k : k + 1, cols] for k in range(taps)]
        ut = [up_taps[k : k + 1, cols] for k in range(taps)]
        gb = gate_bias[:, cols]
        ub = up_bias[:, cols]
        for r in range(0, length, row_tile):
            gpad[PAD + r : PAD + r + row_tile, :] = gpre[b, r : r + row_tile, :].astype(F32)
            upad[PAD + r : PAD + r + row_tile, :] = upre[b, r : r + row_tile, :].astype(F32)
        sums = None
        for r in range(0, length, row_tile):
            start = PAD + r - (taps - 1)
            gs = [gpad[start + k : start + k + row_tile, :] for k in range(taps)]
            us = [upad[start + k : start + k + row_tile, :] for k in range(taps)]
            gm = gs[0] * gt[0]
            um = us[0] * ut[0]
            for k in range(1, taps):
                gm = gm + gs[k] * gt[k]
                um = um + us[k] * ut[k]
            gm = gm + gb
            um = um + ub
            s = jax.nn.sigmoid(gm)
            h = hid[b, r : r + row_tile, :].astype(F32)
            gd = h * um * s * (1.0 + gm * (1.0 - s))
            ud = h * gm * s
            gdel[r : r + row_tile, :] = gd
            udel[r : r + row_tile, :] = ud
            parts = (
                [folded(gd * g) for g in gs]
                + [folded(ud * u) for u in us]
                + [folded(gd), folded(ud)]
            )
            sums = parts if sums is None else [a + p for a, p in zip(sums, parts)]
        for k, part in enumerate(sums):
            small[k : k + 1, cols] = jnp.sum(part, axis=0, keepdims=True)
        for r in range(0, length, row_tile):
            first = r + taps - 1
            gk = gdel[first : first + row_tile, :] * gt[0]
            uk = udel[first : first + row_tile, :] * ut[0]
            for k in range(1, taps):
                first = r + taps - 1 - k
                gk = gk + gdel[first : first + row_tile, :] * gt[k]
                uk = uk + udel[first : first + row_tile, :] * ut[k]
            back[r : r + row_tile, 0:CW] = gk.astype(BF16)
            back[r : r + row_tile, CW : 2 * CW] = uk.astype(BF16)
        block = back[...]
        for q in range(NQ):
            own[b * NQ + q] = jnp.dot(
                tok_t[q * rows_q : (q + 1) * rows_q, :], block, preferred_element_type=F32
            ).astype(BF16)

        @pl.when(b == 0)
        def _():
            for copy in weight_copies:
                copy.wait()

        weights = jnp.concatenate([gw[:, cols], uw[:, cols]], axis=1)
        dot_rows = 256 if length % 256 == 0 else length
        for r in range(0, length, dot_rows):
            acc[r : r + dot_rows, :] += lax.dot_general(
                back[r : r + dot_rows, :],
                weights,
                (((1,), (1,)), ((), ())),
                preferred_element_type=F32,
            )
        return carry

    def right_copy(c):
        return pltpu.make_async_remote_copy(
            src_ref=to_right.at[c],
            dst_ref=from_left.at[c],
            send_sem=send_r.at[c],
            recv_sem=recv_r.at[c],
            device_id={"rep": z + 1},
            device_id_type=MESH,
        )

    def left_copy(c):
        return pltpu.make_async_remote_copy(
            src_ref=to_left.at[c],
            dst_ref=from_right.at[c],
            send_sem=send_l.at[c],
            recv_sem=recv_l.at[c],
            device_id={"rep": z - 1},
            device_id_type=MESH,
        )

    small_right = pltpu.make_async_remote_copy(
        src_ref=small_to_right,
        dst_ref=small_from_left,
        send_sem=small_sem.at[0],
        recv_sem=small_sem.at[1],
        device_id={"rep": z + 1},
        device_id_type=MESH,
    )
    small_left = pltpu.make_async_remote_copy(
        src_ref=small_to_left,
        dst_ref=small_from_right,
        send_sem=small_sem.at[2],
        recv_sem=small_sem.at[3],
        device_id={"rep": z - 1},
        device_id_type=MESH,
    )

    def out_copies(b, q):
        rows = pl.ds(q * rows_q, rows_q)
        return (
            pltpu.make_async_copy(
                out_stage.at[0, q], gate_out.at[rows, columns(b)], out_sem.at[0, q]
            ),
            pltpu.make_async_copy(
                out_stage.at[1, q], up_out.at[rows, columns(b)], out_sem.at[1, q]
            ),
        )

    def scatter_copy(d):
        peer = lax.rem(me + d, tp_count)
        return pltpu.make_async_remote_copy(
            src_ref=term.at[peer],
            dst_ref=term_in.at[d - 1],
            send_sem=scatter_send.at[d - 1],
            recv_sem=scatter_recv.at[d - 1],
            device_id={"tp": peer},
            device_id_type=MESH,
        )

    def gather_copy(d, slot):
        return pltpu.make_async_remote_copy(
            src_ref=final.at[slot],
            dst_ref=final.at[slot],
            send_sem=gather_send.at[d - 1],
            recv_sem=gather_recv.at[d - 1],
            device_id={"tp": lax.rem(me + d, tp_count)},
            device_id_type=MESH,
        )

    term_rows = length // tp_count

    def step(s, carry):
        first = jnp.where(s < warm, s, 2 * s - warm)
        last = jnp.minimum(jnp.where(s < warm, s + 1, 2 * s - warm + 2), blocks)
        lax.fori_loop(first, last, compute, 0)

        b_right = s - z
        b_left = s - (rep_count - 1 - z)
        b_out = s - (rep_count - 1)
        for q in range(NQ):

            @pl.when((b_right >= 0) & (b_right < blocks))
            def _():
                c = b_right * NQ + q

                @pl.when(has_left)
                def _():
                    right_copy(c).wait_recv()

                @pl.when(has_right)
                def _():
                    to_right[c] = (from_left[c].astype(F32) + own[c].astype(F32)).astype(BF16)
                    right_copy(c).start()

            @pl.when((b_left >= 0) & (b_left < blocks))
            def _():
                c = b_left * NQ + q

                @pl.when(has_right)
                def _():
                    left_copy(c).wait_recv()

                @pl.when(has_left)
                def _():
                    to_left[c] = (from_right[c].astype(F32) + own[c].astype(F32)).astype(BF16)
                    left_copy(c).start()

            @pl.when((b_out >= 0) & (b_out < blocks))
            def _():
                c = b_out * NQ + q

                @pl.when(b_out > 0)
                def _():
                    for copy in out_copies(b_out - 1, q):
                        copy.wait()

                total = (
                    from_left[c].astype(F32) + own[c].astype(F32) + from_right[c].astype(F32)
                ).astype(BF16)
                out_stage[0, q] = total[:, 0:CW]
                out_stage[1, q] = total[:, CW : 2 * CW]
                for copy in out_copies(b_out, q):
                    copy.start()

        @pl.when(s == done)
        def _():
            for k in range(tp_count):
                term[k] = acc[k * term_rows : (k + 1) * term_rows, :].astype(BF16)
            for d in range(1, tp_count):
                scatter_copy(d).start()

        @pl.when(s == done + 2)
        def _():
            total = term[me].astype(F32)
            for d in range(1, tp_count):
                scatter_copy(d).wait()
                total = total + term_in[d - 1].astype(F32)
            final[me] = total.astype(BF16)
            for d in range(1, tp_count):
                gather_copy(d, me).start()

        @pl.when(s == done + z)
        def _():
            @pl.when(has_left)
            def _():
                small_right.wait_recv()

            @pl.when(has_right)
            def _():
                small_to_right[...] = small_from_left[...] + small[...]
                small_right.start()

        @pl.when(s == done + rep_count - 1 - z)
        def _():
            @pl.when(has_right)
            def _():
                small_left.wait_recv()

            @pl.when(has_left)
            def _():
                small_to_left[...] = small_from_right[...] + small[...]
                small_left.start()

        return carry

    lax.fori_loop(0, steps, step, 0)

    def final_copy(slot):
        return pltpu.make_async_copy(
            final.at[slot],
            grad_out.at[pl.ds(pl.multiple_of(slot * term_rows, term_rows), term_rows), :],
            final_sem.at[slot],
        )

    final_copy(me).start()
    for d in range(1, tp_count):
        sender = lax.rem(me + tp_count - d, tp_count)
        gather_copy(d, sender).wait_recv()
        final_copy(sender).start()
    for d in range(1, tp_count):
        gather_copy(d, me).wait_send()
    small_out[...] = small_from_left[...] + small[...] + small_from_right[...]

    @pl.when(has_right)
    def _():
        small_right.wait_send()

        def drain(c, carry):
            right_copy(c).wait_send()
            return carry

        lax.fori_loop(0, blocks * NQ, drain, 0)

    @pl.when(has_left)
    def _():
        small_left.wait_send()

        def drain(c, carry):
            left_copy(c).wait_send()
            return carry

        lax.fori_loop(0, blocks * NQ, drain, 0)

    for q in range(NQ):
        for copy in out_copies(blocks - 1, q):
            copy.wait()
    for slot in range(tp_count):
        final_copy(slot).wait()


def per_device(
    rep_count,
    tp_count,
    tokens,
    gate_pre,
    up_pre,
    hidden_grad,
    gate_weight,
    up_weight,
    gate_taps,
    up_taps,
    gate_bias,
    up_bias,
):
    length, hidden_cols = gate_pre.shape
    width = tokens.shape[1]
    taps = gate_taps.shape[0]
    blocks = hidden_cols // CW
    chunks = blocks * NQ
    rows_q = width // NQ
    term_rows = length // tp_count
    small_rows = 2 * taps + 2
    anywhere = pl.BlockSpec(memory_space=pl.ANY)
    vmem = pl.BlockSpec(memory_space=pltpu.VMEM)
    line = pltpu.VMEM((chunks, rows_q, 2 * CW), BF16)
    small = pltpu.VMEM((small_rows, hidden_cols), F32)
    dma = pltpu.SemaphoreType.DMA
    grad, gate_sum, up_sum, small_sum = pl.pallas_call(
        functools.partial(fused, rep_count, tp_count),
        out_shape=(
            jax.ShapeDtypeStruct((length, width), BF16),
            jax.ShapeDtypeStruct((width, hidden_cols), BF16),
            jax.ShapeDtypeStruct((width, hidden_cols), BF16),
            jax.ShapeDtypeStruct((small_rows, hidden_cols), F32),
        ),
        in_specs=[anywhere] * 6 + [vmem] * 4,
        out_specs=(anywhere, anywhere, anywhere, vmem),
        scratch_shapes=[
            pltpu.VMEM((length, width), BF16),
            pltpu.VMEM((width, length), BF16),
            pltpu.VMEM((blocks, length, CW), BF16),
            pltpu.VMEM((blocks, length, CW), BF16),
            pltpu.VMEM((blocks, length, CW), BF16),
            pltpu.VMEM((width, hidden_cols), BF16),
            pltpu.VMEM((width, hidden_cols), BF16),
            pltpu.VMEM((PAD + length, CW), F32),
            pltpu.VMEM((PAD + length, CW), F32),
            pltpu.VMEM((length + PAD, CW), F32),
            pltpu.VMEM((length + PAD, CW), F32),
            pltpu.VMEM((length, 2 * CW), BF16),
            pltpu.VMEM((length, width), F32),
            line,
            line,
            line,
            line,
            line,
            pltpu.VMEM((2, NQ, rows_q, CW), BF16),
            pltpu.VMEM((tp_count, term_rows, width), BF16),
            pltpu.VMEM((tp_count - 1, term_rows, width), BF16),
            pltpu.VMEM((tp_count, term_rows, width), BF16),
            small,
            small,
            small,
            small,
            small,
            dma((3, blocks)),
            dma((3,)),
            dma((chunks,)),
            dma((chunks,)),
            dma((chunks,)),
            dma((chunks,)),
            dma((2, NQ)),
            dma((tp_count - 1,)),
            dma((tp_count - 1,)),
            dma((tp_count - 1,)),
            dma((tp_count - 1,)),
            dma((tp_count,)),
            dma((4,)),
        ],
        compiler_params=pltpu.CompilerParams(
            collective_id=0, has_side_effects=True, vmem_limit_bytes=67043328
        ),
    )(
        tokens,
        gate_pre,
        up_pre,
        hidden_grad,
        gate_weight,
        up_weight,
        gate_taps,
        up_taps,
        gate_bias[None, :],
        up_bias[None, :],
    )
    return (
        grad,
        gate_sum.astype(F32),
        up_sum.astype(F32),
        small_sum[0:taps],
        small_sum[taps : 2 * taps],
        small_sum[2 * taps],
        small_sum[2 * taps + 1],
    )


def solution(mesh):
    return jax.shard_map(
        functools.partial(per_device, mesh.shape["rep"], mesh.shape["tp"]),
        mesh=mesh,
        in_specs=(
            P("rep", "fs"),
            P("rep", "tp"),
            P("rep", "tp"),
            P("rep", "tp"),
            P("fs", "tp"),
            P("fs", "tp"),
            P(None, "tp"),
            P(None, "tp"),
            P("tp"),
            P("tp"),
        ),
        out_specs=(
            P("rep", "fs"),
            P("fs", "tp"),
            P("fs", "tp"),
            P(None, "tp"),
            P(None, "tp"),
            P("tp"),
            P("tp"),
        ),
        check_vma=False,
    )
```

time: 330 us -> 182 us (0.55)
  waiting for transfers between devices: 231 us -> 0 us
  Pallas kernels: 0 us -> 167 us
  blocking collectives: 21.1 us -> 0 us
  other arithmetic: 27.4 us -> 9.19 us
  matrix products: 17 us -> 0 us
  between operations: 15.7 us -> 0.65 us
  local copies, waits for them, and re-layouts: 17.4 us -> 5 us
    psum x1 -> x0, waiting for transfers between devices: 200 us -> none  [per_device(): lax.psum(gate_local.astype(jnp.bfloat16), 'rep').astype(jnp.float32)]
    pallas_call x0 -> x1, Pallas kernels: none -> 167 us  [per_device(): pl.pallas_call(functools.partial(fused, rep_count, tp_count), out_shape=(...]
    reduce_scatter x1 -> x0, waiting for transfers between devices: 30.9 us -> none  [per_device(): lax.psum_scatter(full_partial.astype(jnp.bfloat16), 'tp', scatter_dimensi...]
    psum x1 -> x0, blocking collectives: 21.1 us -> none  [per_device(): lax.psum(gate_tap_part.astype(jnp.bfloat16), 'rep').astype(jnp.float32)]
    dot_general x4 -> x0, matrix products: 17 us -> none  [the longest x1 6.58 us: per_device(): lax.dot_general(tokens, gate_back, token_dims, preferred_element_type=jnp...]
    reduce_sum x2 -> x0, other arithmetic: 16.1 us -> none  [the longest x1 10.3 us: backward_terms(): jnp.sum(gate_delta, axis=0)]
    unnamed x25 -> x7, local copies, waits for them, and re-layouts: 15.4 us -> 1.15 us
    convert_element_type x7 -> x2, other arithmetic: 11.3 us -> 9.19 us  [the longest x1 5.62 us: per_device(): gate_sum.astype(F32)]
  transfers between devices with their start and end apart: 3 -> 0, of which waited for: 2 -> 0; matrix products, arithmetic and copies ran while one was open for 4% -> 0% of each run, Pallas kernels for 0% -> 0%
where the time goes in v1:
time: 182 us
  Pallas kernels  167 us (92%)
  other arithmetic  9.19 us (5%)
  local copies, waits for them, and re-layouts  5 us (3%)
    pallas_call x1, Pallas kernels, per_device(): pl.pallas_call(functools.partial(fused, rep_count, tp_count), out_shape=(...  167 us
    convert_element_type x1, other arithmetic, per_device(): gate_sum.astype(F32)  5.62 us

profile of v1, /device:TPU:0, one launch (start us, length us, event | category | flops | bytes accessed | tf_op | source)
XLA Modules:
  0.0 181.6 jit_solution(9632312667060632935)
XLA Ops:
  0.6 1.3 broadcast_in_dim.6.gate_bias
  1.9 1.3 broadcast_in_dim.7.up_bias
  3.2 166.7 %shard_map.153 = (bf16[768,1024]{1,0:T(8,128)(2,1)}, bf16[1024,1536]{1,0:T(8,128)(2,1)}, bf16[1024,1536]{1,0:T(8,128)(2,1)}, f32[8,1536]{1,0:T(8,128)}) custom-call(bf16[768,1024]{1,0:T(8,128)(2,1)} %tokens.1, bf16[768,1536]{1,0:T(8,128)(2,1)} %gate_pre.1, bf16[768,1536]{1,0:T(8,128)(2,1)} %up_pre.1, bf16[768,1536]{1,0:T(8,128)(2,1)} %hidden.1, ...), custom_call_target="tpu_custom_call" | custom-call | tf_op jit(solution)/shard_map/pallas_call | solution.py:483
  170.0 0.0 copy-start
  170.0 5.6 %convert_element_type.6 = f32[1024,1536]{1,0:T(8,128)} convert(bf16[1024,1536]{1,0:T(8,128)(2,1)} %get-tuple-element.12) | non-fusion elementwise | flops 1572864 | bytes 9437184 | tf_op jit(solution)/shard_map/convert_element_type | solution.py:552
  175.6 0.0 copy-done
  175.6 0.0 copy-start.2
  175.6 0.0 copy-start.1
  175.6 3.6 %convert_element_type.7 = f32[1024,1536]{1,0:T(8,128)} convert(bf16[1024,1536]{1,0:T(8,128)(2,1)S(1)} %copy-done) | non-fusion elementwise | flops 1572864 | bytes 9437184 | tf_op jit(solution)/shard_map/convert_element_type | solution.py:553
  179.2 0.0 copy-done.2
  179.2 0.6 fusion
  179.8 0.6 slice_reduce_fusion
  180.4 0.0 copy-done.1
  180.4 1.1 copy.18
Async XLA Ops:
  170.0 5.6 %copy-start = (bf16[1024,1536]{1,0:T(8,128)(2,1)S(1)}, bf16[1024,1536]{1,0:T(8,128)(2,1)}, u32[]{:S(2)}) copy-start(bf16[1024,1536]{1,0:T(8,128)(2,1)} %get-tuple-element.13) | copy-start | bytes 9437188
  175.6 3.6 %copy-start.2 = (f32[8,1536]{1,0:T(8,128)S(1)}, f32[8,1536]{1,0:T(8,128)}, u32[]{:S(2)}) copy-start(f32[8,1536]{1,0:T(8,128)} %get-tuple-element.14) | copy-start | bytes 147460
  175.6 4.8 %copy-start.1 = (bf16[768,1024]{1,0:T(8,128)(2,1)S(1)}, bf16[768,1024]{1,0:T(8,128)(2,1)}, u32[]{:S(2)}) copy-start(bf16[768,1024]{1,0:T(8,128)(2,1)} %get-tuple-element.26) | copy-start | bytes 4718596

commit v2 on v1

--- a/solution.py
+++ b/solution.py
@@ -9,7 +9,7 @@
 
 MESH = pl.DeviceIdType.MESH
 CW = 128
-NQ = 4
+NQ = 8
 PAD = 8
 F32 = jnp.float32
 BF16 = jnp.bfloat16
@@ -180,8 +180,8 @@
         cols = columns(b)
         gt = [gate_taps[k : k + 1, cols] for k in range(taps)]
         ut = [up_taps[k : k + 1, cols] for k in range(taps)]
-        gb = gate_bias[:, cols]
-        ub = up_bias[:, cols]
+        gb = gate_bias[cols].reshape(1, CW)
+        ub = up_bias[cols].reshape(1, CW)
         for r in range(0, length, row_tile):
             gpad[PAD + r : PAD + r + row_tile, :] = gpre[b, r : r + row_tile, :].astype(F32)
             upad[PAD + r : PAD + r + row_tile, :] = upre[b, r : r + row_tile, :].astype(F32)
@@ -544,8 +544,8 @@
         up_weight,
         gate_taps,
         up_taps,
-        gate_bias[None, :],
-        up_bias[None, :],
+        gate_bias,
+        up_bias,
     )
     return (
         grad,

time: 182 us -> 181 us (level)
  local copies, waits for them, and re-layouts: 5 us -> 2.41 us
  Pallas kernels: 167 us -> 169 us
    broadcast_in_dim x2 -> x0, local copies, waits for them, and re-layouts: 2.59 us -> none  [the longest x1 1.3 us: per_device(): gate_bias[None, :]]
where the time goes in v2:
time: 181 us
  Pallas kernels  169 us (93%)
  other arithmetic  9.19 us (5%)
  local copies, waits for them, and re-layouts  2.41 us (1%)
    pallas_call x1, Pallas kernels, per_device(): pl.pallas_call(functools.partial(fused, rep_count, tp_count), out_shape=(...  169 us
    convert_element_type x1, other arithmetic, per_device(): gate_sum.astype(F32)  5.62 us

profile of v2, /device:TPU:0, one launch (start us, length us, event | category | flops | bytes accessed | tf_op | source)
XLA Modules:
  0.0 180.8 jit_solution(7863464995203314822)
XLA Ops:
  0.6 168.6 %shard_map.153 = (bf16[768,1024]{1,0:T(8,128)(2,1)}, bf16[1024,1536]{1,0:T(8,128)(2,1)}, bf16[1024,1536]{1,0:T(8,128)(2,1)}, f32[8,1536]{1,0:T(8,128)}) custom-call(bf16[768,1024]{1,0:T(8,128)(2,1)} %tokens.1, bf16[768,1536]{1,0:T(8,128)(2,1)} %gate_pre.1, bf16[768,1536]{1,0:T(8,128)(2,1)} %up_pre.1, bf16[768,1536]{1,0:T(8,128)(2,1)} %hidden.1, ...), custom_call_target="tpu_custom_call" | custom-call | tf_op jit(solution)/shard_map/pallas_call | solution.py:483
  169.2 0.0 copy-start
  169.2 5.6 %convert_element_type.6 = f32[1024,1536]{1,0:T(8,128)} convert(bf16[1024,1536]{1,0:T(8,128)(2,1)} %get-tuple-element.12) | non-fusion elementwise | flops 1572864 | bytes 9437184 | tf_op jit(solution)/shard_map/convert_element_type | solution.py:552
  174.8 0.0 copy-done
  174.8 0.0 copy-start.2
  174.8 0.0 copy-start.1
  174.8 3.6 %convert_element_type.7 = f32[1024,1536]{1,0:T(8,128)} convert(bf16[1024,1536]{1,0:T(8,128)(2,1)S(1)} %copy-done) | non-fusion elementwise | flops 1572864 | bytes 9437184 | tf_op jit(solution)/shard_map/convert_element_type | solution.py:553
  178.4 0.0 copy-done.2
  178.4 0.6 fusion
  179.0 0.6 slice_reduce_fusion
  179.7 0.0 copy-done.1
  179.7 1.1 copy.18
Async XLA Ops:
  169.2 5.6 %copy-start = (bf16[1024,1536]{1,0:T(8,128)(2,1)S(1)}, bf16[1024,1536]{1,0:T(8,128)(2,1)}, u32[]{:S(2)}) copy-start(bf16[1024,1536]{1,0:T(8,128)(2,1)} %get-tuple-element.13) | copy-start | bytes 9437188
  174.8 3.6 %copy-start.2 = (f32[8,1536]{1,0:T(8,128)S(1)}, f32[8,1536]{1,0:T(8,128)}, u32[]{:S(2)}) copy-start(f32[8,1536]{1,0:T(8,128)} %get-tuple-element.14) | copy-start | bytes 147460
  174.8 4.8 %copy-start.1 = (bf16[768,1024]{1,0:T(8,128)(2,1)S(1)}, bf16[768,1024]{1,0:T(8,128)(2,1)}, u32[]{:S(2)}) copy-start(bf16[768,1024]{1,0:T(8,128)(2,1)} %get-tuple-element.26) | copy-start | bytes 4718596
